TPU v7x, 32 devices: a whole 2x2x4 slice. The times are simulated.
32 devices in a mesh: ep: 8 (over z, y), tp: 4 (over x, core).
Axes of the slice: x: 2, y: 2, z: 4, core: 2. Of those that a mesh axis runs over, the one named last changes fastest.
Arguments:
- queries: bfloat16 [4096, 1024], P('ep', 'tp'), may hold values from -6 to 6
- keys: bfloat16 [4096, 512], P('ep', 'tp'), may hold values from -6 to 6
- values: bfloat16 [4096, 512], P('ep', 'tp'), may hold values from -384 to 384
- query_gain: float32 [128], replicated, may hold values from 0.1 to 1.9
- key_gain: float32 [128], replicated, may hold values from 0.1 to 1.9
- out_proj: bfloat16 [1024, 2048], replicated, may hold values from -0.1875 to 0.1875
- tokens_b: bfloat16 [4096, 2048], P(('ep', 'tp')), may hold values from -6 to 6
- norm_gain: float32 [2048], replicated, may hold values from 0.1 to 1.9
- routes: int32 [4096, 2], P(('ep', 'tp')), may hold values from 0 to 31, all different within a row; in each aligned block of 128 rows (0 to 127, 128 to 255, ...) at most 16 rows name the same one
- group_prob: float32 [4096], P(('ep', 'tp')), may hold values from 0.25 to 1
- expert_logits: float32 [4096, 2], P(('ep', 'tp')), may hold values from -6 to 6
- w_gate: bfloat16 [32, 2048, 512], P(('ep', 'tp')), may hold values from -0.125 to 0.125
- w_up: bfloat16 [32, 2048, 512], P(('ep', 'tp')), may hold values from -0.125 to 0.125
- w_down: bfloat16 [32, 512, 2048], P(('ep', 'tp')), may hold values from -0.25 to 0.25
Outputs:
- mixed_a: bfloat16 [4096, 2048], P(('ep', 'tp'))
- mixed_b: bfloat16 [4096, 2048], P(('ep', 'tp'))
Inputs may be any that keep to these rules, and one draw needn't show every extreme that they name: Within the 128 rows of one device, no expert is named by more than 16 of the routes, and in every draw some expert is named exactly 16 times by the rows of some device. The 2 experts of a row differ.
All inputs are finite; a program needn't handle non-finite values.
Results may differ from a plain program's by a relative error of at most 0.014.
Values may be sent and summed in bfloat16 or wider, within the bound.
A program may use at most 128 MiB of HBM per device.

v0:
```python
import math

import jax
import jax.numpy as jnp
from jax import lax
from jax.sharding import PartitionSpec as P

GRID_W = 64


NORM_EPS = 1e-06
ROPE_BASE = 10000.0


def rope_angles(row_count, offset, head_dim):
    quarter = head_dim // 4
    position = offset + jnp.arange(row_count, dtype=jnp.int32)
    grid_row = (position // GRID_W).astype(jnp.float32)
    grid_col = (position % GRID_W).astype(jnp.float32)
    frequency = ROPE_BASE ** (-jnp.arange(quarter, dtype=jnp.float32) / quarter)
    angles = jnp.concatenate([grid_row[:, None] * frequency, grid_col[:, None] * frequency], axis=1)
    return (jnp.cos(angles), jnp.sin(angles))


def norm_rotate(block_in, gain, cos_table, sin_table):
    wide = block_in.astype(jnp.float32)
    wide = wide * lax.rsqrt(jnp.mean(wide * wide, axis=-1, keepdims=True) + NORM_EPS) * gain
    half_width = wide.shape[-1] // 2
    first_half, second_half = (wide[..., :half_width], wide[..., half_width:])
    cos_b = cos_table[:, None, :]
    sin_b = sin_table[:, None, :]
    turned = jnp.concatenate(
        [first_half * cos_b - second_half * sin_b, second_half * cos_b + first_half * sin_b],
        axis=-1,
    )
    return turned.astype(jnp.bfloat16)


def attention_half(queries, keys, values, query_gain, key_gain, out_proj):
    row_count = queries.shape[0]
    head_dim = query_gain.shape[0]
    local_heads = queries.shape[1] // head_dim
    local_kv = keys.shape[1] // head_dim
    group_size = local_heads // local_kv
    offset = lax.axis_index("ep") * row_count
    cos_table, sin_table = rope_angles(row_count, offset, head_dim)
    qrot = norm_rotate(
        queries.reshape(row_count, local_heads, head_dim), query_gain, cos_table, sin_table
    )
    qrot = qrot.reshape(row_count, local_kv, group_size, head_dim)
    krot = norm_rotate(keys.reshape(row_count, local_kv, head_dim), key_gain, cos_table, sin_table)
    krot = krot.reshape(row_count, local_kv * head_dim)
    score_scale = head_dim ** (-0.5)
    start_pair = (
        jnp.zeros((row_count, local_kv, group_size, head_dim), jnp.float32),
        jnp.zeros((row_count, local_kv, group_size), jnp.float32),
    )
    key_piece = lax.all_gather(krot, "ep", axis=0, tiled=True)
    value_piece = lax.all_gather(values, "ep", axis=0, tiled=True)
    piece_rows = key_piece.shape[0]
    key_block = math.gcd(piece_rows, 1024)
    block_count = piece_rows // key_block
    key_tiles = key_piece.reshape(block_count, key_block, local_kv, head_dim)
    value_tiles = value_piece.reshape(block_count, key_block, local_kv, head_dim)

    def key_step(pair, tiles):
        numerator, denominator = pair
        key_tile, value_tile = tiles
        scores = (
            jnp.einsum("qhgd,khd->qhgk", qrot, key_tile, preferred_element_type=jnp.float32)
            * score_scale
        )
        weights = jnp.exp(scores).astype(jnp.bfloat16)
        denominator = denominator + jnp.sum(weights.astype(jnp.float32), axis=-1)
        numerator = numerator + jnp.einsum(
            "qhgk,khd->qhgd", weights, value_tile, preferred_element_type=jnp.float32
        )
        return ((numerator, denominator), None)

    numerator, denominator = lax.scan(key_step, start_pair, (key_tiles, value_tiles))[0]
    attended = (
        (numerator / denominator[..., None])
        .astype(jnp.bfloat16)
        .reshape(row_count, local_heads * head_dim)
    )
    own_width = local_heads * head_dim
    own_rows = lax.dynamic_slice_in_dim(out_proj, lax.axis_index("tp") * own_width, own_width, 0)
    return lax.psum_scatter(
        jnp.dot(attended, own_rows, preferred_element_type=jnp.float32).astype(jnp.bfloat16),
        "tp",
        scatter_dimension=0,
        tiled=True,
    )


def expert_apply(inputs, gate_w, up_w, down_w):
    gate_part = jnp.dot(inputs, gate_w, preferred_element_type=jnp.float32)
    up_part = jnp.dot(inputs, up_w, preferred_element_type=jnp.float32)
    hidden = (jax.nn.silu(gate_part) * up_part).astype(jnp.bfloat16)
    return jnp.dot(hidden, down_w, preferred_element_type=jnp.float32).astype(jnp.bfloat16)


def expert_half(tokens_b, norm_gain, routes, group_prob, expert_logits, w_gate, w_up, w_down):
    ep_count = lax.axis_size("ep")
    tp_count = lax.axis_size("tp")
    device_count = ep_count * tp_count
    row_count, top_count = routes.shape
    model_width = tokens_b.shape[1]
    capacity = 2 * top_count * row_count // device_count
    wide_b = tokens_b.astype(jnp.float32)
    normed = (
        wide_b * lax.rsqrt(jnp.mean(wide_b * wide_b, axis=-1, keepdims=True) + NORM_EPS) * norm_gain
    ).astype(jnp.bfloat16)
    flat_routes = routes.reshape(-1)
    onehot = (flat_routes[:, None] == jnp.arange(device_count, dtype=jnp.int32)[None, :]).astype(
        jnp.int32
    )
    slot_rank = jnp.sum((jnp.cumsum(onehot, axis=0) - onehot) * onehot, axis=1)
    target_slot = flat_routes * capacity + slot_rank
    token_index = jnp.arange(row_count * top_count, dtype=jnp.int32) // top_count
    sender = (
        jnp.zeros((device_count * capacity, model_width), jnp.bfloat16)
        .at[target_slot]
        .set(normed[token_index])
    )
    arrived = lax.all_to_all(
        sender.reshape(device_count, capacity, model_width),
        ("ep", "tp"),
        split_axis=0,
        concat_axis=0,
        tiled=True,
    )
    expert_out = expert_apply(
        arrived.reshape(device_count * capacity, model_width), w_gate[0], w_up[0], w_down[0]
    )
    returned = lax.all_to_all(
        expert_out.reshape(device_count, capacity, model_width),
        ("ep", "tp"),
        split_axis=0,
        concat_axis=0,
        tiled=True,
    )
    returned = returned.reshape(device_count * capacity, model_width)
    picked = returned[target_slot].reshape(row_count, top_count, model_width).astype(jnp.float32)
    combine = group_prob[:, None] * jax.nn.softmax(expert_logits, axis=-1)
    return jnp.sum(picked * combine[:, :, None], axis=1).astype(jnp.bfloat16)


def body(
    queries,
    keys,
    values,
    query_gain,
    key_gain,
    out_proj,
    tokens_b,
    norm_gain,
    routes,
    group_prob,
    expert_logits,
    w_gate,
    w_up,
    w_down,
):
    mixed_a = attention_half(queries, keys, values, query_gain, key_gain, out_proj)
    mixed_b = expert_half(
        tokens_b, norm_gain, routes, group_prob, expert_logits, w_gate, w_up, w_down
    )
    return (mixed_a, mixed_b)


def solution(mesh):
    placed = (
        P("ep", "tp"),
        P("ep", "tp"),
        P("ep", "tp"),
        P(),
        P(),
        P(),
        P(("ep", "tp"), None),
        P(),
        P(("ep", "tp"), None),
        P(("ep", "tp")),
        P(("ep", "tp"), None),
        P(("ep", "tp"), None, None),
        P(("ep", "tp"), None, None),
        P(("ep", "tp"), None, None),
    )
    return jax.shard_map(
        body,
        mesh=mesh,
        in_specs=placed,
        out_specs=(P(("ep", "tp"), None), P(("ep", "tp"), None)),
        check_vma=False,
    )
```

profile of v0, /device:TPU:0, one launch (start us, length us, event | category | flops | bytes accessed | tf_op | source)
XLA Modules:
  0.0 214.3 jit_solution(13210312035628791452)
XLA Ops:
  7.2 0.0 copy-start
  7.2 0.0 copy-start.5
  7.2 0.0 copy-start.1
  7.2 0.0 copy-start.4
  7.2 0.0 all-gather.5.cloned.1.call-start
  7.3 1.2 copy.30
  8.5 0.7 fusion.40
  9.3 0.1 broadcast_multiply_fusion.1
  9.4 0.5 fusion.47
  9.9 0.7 pad_maximum_fusion.2
  10.5 0.0 all-gather.5.cloned.1.call-update
  10.5 0.0 all-gather.3.cloned.1.call-start
  10.6 0.7 all-gather.3.cloned.1.call-update
  11.3 0.0 copy-done.5
  11.3 0.1 copy.36
  11.4 0.1 eq.31
  11.6 0.1 eq.27
  11.7 0.6 reduce-window.6
  12.3 0.2 slice_reduce_fusion
  12.6 0.1 copy.35
  12.7 0.1 mul.229
  12.8 0.0 copy-done.1
  12.8 0.2 fusion.26
  13.0 0.1 fusion.51
  13.2 0.0 copy-done.4
  13.2 0.2 fusion.28
  13.4 7.0 %scatter_custom_fusion = bf16[512,2048]{1,0:T(8,128)(2,1)} fusion(s32[256]{0:T(256)S(1)} %bitcast.124, bf16[128,2048]{1,0:T(8,128)(2,1)S(1)} %fusion.28, s32[1024]{0:T(1024)S(1)} %pad_clamp_fusion.1, bf16[]{:T(256)} %constant.102.clone.1), kind=kCustom, calls=%fused_computation.32 | custom fusion | bytes 2097154 | tf_op jit(solution)/shard_map/scatter | solution.py:124
  20.4 7.6 %all-to-all-start = ((bf16[32,16,2048]{2,1,0:T(8,128)(2,1)}), bf16[32,16,2048]{2,1,0:T(8,128)(2,1)}, u32[]{:S(2)}, u32[]{:S(2)}) async-start(bf16[32,16,2048]{2,1,0:T(8,128)(2,1)} %bitcast.118), calls=%async_computation.1 | async-start | bytes 4194304 | tf_op jit(solution)/shard_map/all_to_all | solution.py:126
  28.0 0.0 copy-done.2
  28.0 0.1 copy.31
  28.2 0.5 fusion.44
  28.7 0.1 fusion.35
  28.7 0.0 copy-done.7
  28.8 0.1 fusion.36
  28.9 0.1 fusion.41
  29.0 0.2 copy.34
  29.2 39.7 %all-gather.5.cloned.1.call-done = bf16[4096,128]{0,1:T(8,128)(2,1)} async-done(((bf16[512,128]{0,1:T(8,128)(2,1)}), bf16[4096,128]{0,1:T(8,128)(2,1)}) %all-gather.5.cloned.1.call-update) | async-done | bytes 1048592 | tf_op jit(solution)/shard_map/all_gather | solution.py:58
  68.8 2.3 %copy.41 = bf16[4096,128]{1,0:T(8,128)(2,1)} copy(bf16[4096,128]{0,1:T(8,128)(2,1)} %all-gather.5.cloned.1.call-done) | data formatting | bytes 2097152
  71.1 40.1 %all-gather.3.cloned.1.call-done = bf16[4096,128]{1,0:T(8,128)(2,1)} async-done(((bf16[512,128]{1,0:T(8,128)(2,1)}), bf16[4096,128]{1,0:T(8,128)(2,1)}) %all-gather.3.cloned.1.call-update) | async-done | bytes 1048592 | tf_op jit(solution)/shard_map/all_gather | solution.py:59
  111.2 21.3 %while.13 = (s32[]{:T(128)}, f32[512,1,2,128]{0,3,2,1:T(8,128)S(1)}, f32[512,1,2]{0,2,1:T(2,128)S(1)}, bf16[4,1024,1,128]{3,1,0,2:T(8,128)(2,1)}, bf16[4,1024,1,...) while((s32[]{:T(128)}, ...), condition=%wide.region_4.5_spmd.clone, body=%wide.region_2.4_spmd.clone.sunk | while | flops 541328384 | bytes 6046816 | solution.py:80
  111.2 3.1 %convert_reduce_fusion.2 = (f32[512,2]{0,1:T(2,128)S(1)}, bf16[1024,512,2]{1,0,2:T(8,128)(2,1)}) fusion(bf16[512,1,2,128]{3,0,2,1:T(8,128)(2,1)S(1)} %get-tuple-element.160, bf16[4,1024,1,128]{3,1,2,0:T(8,128)(2,1)} %get-tuple-element.159, s32[]{:T(128)} %get-tuple-element.147), kind=kOutput, calls=%fused_computation.3.clone.1 | convolution fusion | flops 272628736 | bytes 2626048 | tf_op jit(solution)/shard_map/while/body/eval_jaxpr/qhgd,khd->qhgk/dot_general | solution.py:70
  114.3 2.2 %fusion.71 = f32[512,1,2,128]{0,3,2,1:T(8,128)S(1)} fusion(bf16[1024,512,2]{1,0,2:T(8,128)(2,1)} %get-tuple-element.137, f32[512,1,2,128]{0,3,2,1:T(8,128)S(1)} %get-tuple-element.148, bf16[4,1024,1,128]{3,1,0,2:T(8,128)(2,1)} %get-tuple-element.158, s32[]{:T(128)} %get-tuple-element.147, pred[]{:T(512)S(6)} %compare.18), kind=kOutput, calls=%fused_computation.8.clone.1 | convolution fusion | flops 268697600 | bytes 3408385 | tf_op jit(solution)/shard_map/while/body/eval_jaxpr/qhgk,khd->qhgd/dot_general | solution.py:75
  116.6 3.1 %convert_reduce_fusion.2 = (f32[512,2]{0,1:T(2,128)S(1)}, bf16[1024,512,2]{1,0,2:T(8,128)(2,1)}) fusion(bf16[512,1,2,128]{3,0,2,1:T(8,128)(2,1)S(1)} %get-tuple-element.160, bf16[4,1024,1,128]{3,1,2,0:T(8,128)(2,1)} %get-tuple-element.159, s32[]{:T(128)} %get-tuple-element.147), kind=kOutput, calls=%fused_computation.3.clone.1 | convolution fusion | flops 272628736 | bytes 2626048 | tf_op jit(solution)/shard_map/while/body/eval_jaxpr/qhgd,khd->qhgk/dot_general | solution.py:70
  119.7 2.2 %fusion.71 = f32[512,1,2,128]{0,3,2,1:T(8,128)S(1)} fusion(bf16[1024,512,2]{1,0,2:T(8,128)(2,1)} %get-tuple-element.137, f32[512,1,2,128]{0,3,2,1:T(8,128)S(1)} %get-tuple-element.148, bf16[4,1024,1,128]{3,1,0,2:T(8,128)(2,1)} %get-tuple-element.158, s32[]{:T(128)} %get-tuple-element.147, pred[]{:T(512)S(6)} %compare.18), kind=kOutput, calls=%fused_computation.8.clone.1 | convolution fusion | flops 268697600 | bytes 3408385 | tf_op jit(solution)/shard_map/while/body/eval_jaxpr/qhgk,khd->qhgd/dot_general | solution.py:75
  121.9 3.1 %convert_reduce_fusion.2 = (f32[512,2]{0,1:T(2,128)S(1)}, bf16[1024,512,2]{1,0,2:T(8,128)(2,1)}) fusion(bf16[512,1,2,128]{3,0,2,1:T(8,128)(2,1)S(1)} %get-tuple-element.160, bf16[4,1024,1,128]{3,1,2,0:T(8,128)(2,1)} %get-tuple-element.159, s32[]{:T(128)} %get-tuple-element.147), kind=kOutput, calls=%fused_computation.3.clone.1 | convolution fusion | flops 272628736 | bytes 2626048 | tf_op jit(solution)/shard_map/while/body/eval_jaxpr/qhgd,khd->qhgk/dot_general | solution.py:70
  125.0 2.2 %fusion.71 = f32[512,1,2,128]{0,3,2,1:T(8,128)S(1)} fusion(bf16[1024,512,2]{1,0,2:T(8,128)(2,1)} %get-tuple-element.137, f32[512,1,2,128]{0,3,2,1:T(8,128)S(1)} %get-tuple-element.148, bf16[4,1024,1,128]{3,1,0,2:T(8,128)(2,1)} %get-tuple-element.158, s32[]{:T(128)} %get-tuple-element.147, pred[]{:T(512)S(6)} %compare.18), kind=kOutput, calls=%fused_computation.8.clone.1 | convolution fusion | flops 268697600 | bytes 3408385 | tf_op jit(solution)/shard_map/while/body/eval_jaxpr/qhgk,khd->qhgd/dot_general | solution.py:75
  127.2 3.1 %convert_reduce_fusion.2 = (f32[512,2]{0,1:T(2,128)S(1)}, bf16[1024,512,2]{1,0,2:T(8,128)(2,1)}) fusion(bf16[512,1,2,128]{3,0,2,1:T(8,128)(2,1)S(1)} %get-tuple-element.160, bf16[4,1024,1,128]{3,1,2,0:T(8,128)(2,1)} %get-tuple-element.159, s32[]{:T(128)} %get-tuple-element.147), kind=kOutput, calls=%fused_computation.3.clone.1 | convolution fusion | flops 272628736 | bytes 2626048 | tf_op jit(solution)/shard_map/while/body/eval_jaxpr/qhgd,khd->qhgk/dot_general | solution.py:70
  130.3 2.2 %fusion.71 = f32[512,1,2,128]{0,3,2,1:T(8,128)S(1)} fusion(bf16[1024,512,2]{1,0,2:T(8,128)(2,1)} %get-tuple-element.137, f32[512,1,2,128]{0,3,2,1:T(8,128)S(1)} %get-tuple-element.148, bf16[4,1024,1,128]{3,1,0,2:T(8,128)(2,1)} %get-tuple-element.158, s32[]{:T(128)} %get-tuple-element.147, pred[]{:T(512)S(6)} %compare.18), kind=kOutput, calls=%fused_computation.8.clone.1 | convolution fusion | flops 268697600 | bytes 3408385 | tf_op jit(solution)/shard_map/while/body/eval_jaxpr/qhgk,khd->qhgd/dot_general | solution.py:75
  132.6 0.1 divide_convert_fusion
  132.6 0.0 all-to-all-done
  132.6 4.4 %fusion.18 = f32[512,512]{1,0:T(8,128)} fusion(bf16[512,2048]{1,0:T(8,128)(2,1)} %bitcast.18, bf16[1,2048,512]{2,1,0:T(8,128)(2,1)} %param.27), kind=kOutput, calls=%fused_computation.22 | convolution fusion | flops 1073741824 | bytes 5242880 | tf_op jit(solution)/shard_map/dot_general | solution.py:97
  137.1 0.0 copy-done
  137.1 6.2 %convolution_convert_fusion.1 = bf16[512,2048]{1,0:T(8,128)(2,1)} fusion(bf16[1,512,2048]{2,1,0:T(8,128)(2,1)S(1)} %copy-done, bf16[512,2048]{1,0:T(8,128)(2,1)} %bitcast.18, bf16[1,2048,512]{2,1,0:T(8,128)(2,1)} %param.28, f32[512,512]{1,0:T(8,128)} %fusion.18), kind=kOutput, calls=%fused_computation.18 | convolution fusion | flops 2150105088 | bytes 9437184 | tf_op jit(solution)/shard_map/dot_general | solution.py:100
  143.3 3.5 %all-to-all-start.1 = ((bf16[32,16,2048]{2,1,0:T(8,128)(2,1)}), bf16[32,16,2048]{2,1,0:T(8,128)(2,1)}, u32[]{:S(2)}, u32[]{:S(2)}) async-start(bf16[32,16,2048]{2,1,0:T(8,128)(2,1)} %bitcast.119), calls=%async_computation.2 | async-start | bytes 4194304 | tf_op jit(solution)/shard_map/all_to_all | solution.py:136
  146.8 0.3 reduce-scatter.2.cloned.1.call-start
  147.1 3.3 %convolution_convert_fusion = bf16[512,2048]{1,0:T(8,128)(2,1)} fusion(bf16[512,256]{0,1:T(8,128)(2,1)S(1)} %bitcast.121, bf16[1024,2048]{1,0:T(8,128)(2,1)} %param.21, s32[]{:T(128)S(6)} %select_n.58), kind=kOutput, calls=%fused_computation.17 | convolution fusion | flops 537919488 | bytes 3407876 | tf_op jit(solution)/shard_map/dot_general | solution.py:89
  150.4 0.0 reduce-scatter.2.cloned.1.call-update
  150.4 0.7 copy-done.3
  151.1 0.0 copy-done.6
  151.1 0.1 copy.39
  151.2 44.4 %all-to-all-done.1 = bf16[32,16,2048]{2,1,0:T(8,128)(2,1)} async-done(((bf16[32,16,2048]{2,1,0:T(8,128)(2,1)}), bf16[32,16,2048]{2,1,0:T(8,128)(2,1)}, u32[]{:S(2)}, u32[]{:S(2)}) %all-to-all-start.1) | async-done | bytes 2097184 | tf_op jit(solution)/shard_map/all_to_all | solution.py:136
  195.6 4.2 %gather_fusion = bf16[256,2048]{1,0:T(8,128)(2,1)S(1)} fusion(bf16[512,2048]{1,0:T(8,128)(2,1)} %bitcast.23, s32[1024]{0:T(1024)S(1)} %pad_clamp_fusion), kind=kCustom, calls=%fused_computation.1 | custom fusion | bytes 2098176 | tf_op jit(solution)/shard_map/gather | solution.py:144
  199.8 2.3 %reshape.420 = f32[128,2,2048]{2,1,0:T(2,128)} reshape(bf16[256,2048]{1,0:T(8,128)(2,1)S(1)} %gather_fusion) | data formatting | bytes 3145728 | tf_op jit(solution)/shard_map/convert_element_type | solution.py:144
  202.2 5.6 %multiply_reduce_fusion = bf16[128,2048]{1,0:T(8,128)(2,1)} fusion(f32[128,2,2048]{2,1,0:T(2,128)} %reshape.420, f32[128,2]{1,0:T(8,128)S(1)} %copy.39), kind=kLoop, calls=%fused_computation.24 | loop fusion | flops 786432 | bytes 2622464 | tf_op jit(solution)/shard_map/reduce_sum | solution.py:146
  (29 shorter events, 0.3 us)
Async XLA Ops:
  7.2 129.9 %copy-start = (bf16[1,512,2048]{2,1,0:T(8,128)(2,1)S(1)}, bf16[1,512,2048]{2,1,0:T(8,128)(2,1)}, u32[]{:S(2)}) copy-start(bf16[1,512,2048]{2,1,0:T(8,128)(2,1)} %param.29) | copy-start | bytes 6291460
  7.2 4.1 %copy-start.5 = (s32[128,2]{0,1:T(2,128)S(1)}, s32[128,2]{0,1:T(2,128)}, u32[]{:S(2)}) copy-start(s32[128,2]{0,1:T(2,128)} %param.24) | copy-start | bytes 3076
  7.2 5.7 %copy-start.1 = (bf16[128,2048]{1,0:T(8,128)(2,1)S(1)}, bf16[128,2048]{1,0:T(8,128)(2,1)}, u32[]{:S(2)}) copy-start(bf16[128,2048]{1,0:T(8,128)(2,1)} %param.22) | copy-start | bytes 1572868
  7.2 6.0 %copy-start.4 = (f32[2048]{0:T(1024)S(1)}, f32[2048]{0:T(1024)}, u32[]{:S(2)}) copy-start(f32[2048]{0:T(1024)} %param.23) | copy-start | bytes 24580
  7.2 61.6 %all-gather.5.cloned.1.call-start = ((), (), s32[]{:S(2)}) async-start(), calls=%async_computation.4 | async-start | bytes 1179648 | tf_op jit(solution)/shard_map/all_gather | solution.py:58
  10.5 100.7 %all-gather.3.cloned.1.call-start = ((), (), s32[]{:S(2)}) async-start(), calls=%async_computation.3 | async-start | bytes 1179648 | tf_op jit(solution)/shard_map/all_gather | solution.py:59
  20.4 7.7 %copy-start.2 = (bf16[512,256]{1,0:T(8,128)(2,1)S(1)}, bf16[512,256]{1,0:T(8,128)(2,1)}, u32[]{:S(2)}) copy-start(bf16[512,256]{1,0:T(8,128)(2,1)} %param.16) | copy-start | bytes 786436
  20.4 8.4 %copy-start.7 = (f32[128]{0:T(128)S(1)}, f32[128]{0:T(128)}, u32[]{:S(2)}) copy-start(f32[128]{0:T(128)} %param.19) | copy-start | bytes 1540
  20.4 112.2 %all-to-all-start = ((bf16[32,16,2048]{2,1,0:T(8,128)(2,1)}), bf16[32,16,2048]{2,1,0:T(8,128)(2,1)}, u32[]{:S(2)}, u32[]{:S(2)}) async-start(bf16[32,16,2048]{2,1,0:T(8,128)(2,1)} %bitcast.118), calls=%async_computation.1 | async-start | bytes 4194304 | tf_op jit(solution)/shard_map/all_to_all | solution.py:126
  143.3 52.3 %all-to-all-start.1 = ((bf16[32,16,2048]{2,1,0:T(8,128)(2,1)}), bf16[32,16,2048]{2,1,0:T(8,128)(2,1)}, u32[]{:S(2)}, u32[]{:S(2)}) async-start(bf16[32,16,2048]{2,1,0:T(8,128)(2,1)} %bitcast.119), calls=%async_computation.2 | async-start | bytes 4194304 | tf_op jit(solution)/shard_map/all_to_all | solution.py:136
  146.8 61.0 %reduce-scatter.2.cloned.1.call-start = ((), (), s32[]{:S(2)}) async-start(), calls=%async_computation.5 | async-start | bytes 2621440 | tf_op jit(solution)/shard_map/reduce_scatter | solution.py:88
  150.4 0.7 copy-start.3
  150.4 0.7 copy-start.6
Sparse Core Ops, SparseCore 0:
  10.7 58.1 all-gather.4
  71.0 40.2 all-gather.2
  150.7 36.8 reduce-scatter.1
where the time goes:
time: 215 us; the launch traced here: 214 us
  waiting for transfers between devices  125 us (58%)
  matrix products  35.1 us (16%)
  local copies, waits for them, and re-layouts  18.9 us (9%)
  between operations  14 us (7%)
  starting transfers between devices  11.5 us (5%)
  other arithmetic  9.72 us (5%)
    all_to_all x1, waiting for transfers between devices, expert_half(): lax.all_to_all(expert_out.reshape(device_count, capacity, model_width), (...  44.4 us
    all_gather x1, waiting for transfers between devices, attention_half(): value_piece = lax.all_gather(values, 'ep', axis=0, tiled=True)  40.1 us
    all_gather x1, waiting for transfers between devices, attention_half(): key_piece = lax.all_gather(krot, 'ep', axis=0, tiled=True)  39.7 us
    dot_general x4, matrix products, key_step(): jnp.einsum('qhgd,khd->qhgk', qrot, key_tile, preferred_element_type=jnp.f...  12.4 us
    dot_general x4, matrix products, key_step(): jnp.einsum('qhgk,khd->qhgd', weights, value_tile, preferred_element_type=...  8.77 us
    all_to_all x1, starting transfers between devices, expert_half(): lax.all_to_all(sender.reshape(device_count, capacity, model_width), ('ep'...  7.63 us
    scatter x1, local copies, waits for them, and re-layouts, expert_half(): sender = jnp.zeros((device_count * capacity, model_width), jnp.bfloat16)....  7 us
    dot_general x1, matrix products, expert_apply(): jnp.dot(hidden, down_w, preferred_element_type=jnp.float32)  6.21 us
  transfers between devices with their start and end apart: 5, of which 3 were waited for; matrix products, arithmetic and copies ran while one was open for 23% of the time, Pallas kernels for 0%

commit v1 on v0

v1 whole, which is shorter than its diff:
```python
import functools
import math

import jax
import jax.numpy as jnp
from jax import lax
from jax.experimental import pallas as pl
from jax.experimental.pallas import tpu as pltpu
from jax.sharding import PartitionSpec as P

GRID_W = 64


NORM_EPS = 1e-06
ROPE_BASE = 10000.0
VMEM = pl.BlockSpec(memory_space=pltpu.VMEM)


def rope_angles(row_count, offset, head_dim):
    quarter = head_dim // 4
    position = offset + jnp.arange(row_count, dtype=jnp.int32)
    grid_row = (position // GRID_W).astype(jnp.float32)
    grid_col = (position % GRID_W).astype(jnp.float32)
    frequency = ROPE_BASE ** (-jnp.arange(quarter, dtype=jnp.float32) / quarter)
    angles = jnp.concatenate([grid_row[:, None] * frequency, grid_col[:, None] * frequency], axis=1)
    return (jnp.cos(angles), jnp.sin(angles))


def norm_rotate(wide, gain, cos_table, sin_table):
    wide = wide * lax.rsqrt(jnp.mean(wide * wide, axis=-1, keepdims=True) + NORM_EPS) * gain
    half_width = wide.shape[-1] // 2
    first_half, second_half = (wide[..., :half_width], wide[..., half_width:])
    return jnp.concatenate(
        [
            first_half * cos_table - second_half * sin_table,
            second_half * cos_table + first_half * sin_table,
        ],
        axis=-1,
    )


def gather_pieces(block):
    count = lax.axis_size("ep")
    rows = block.shape[0]
    if count % 2 or count < 4:
        return [lax.all_gather(block, "ep", axis=0, tiled=True)]
    partner = lax.ppermute(block, "ep", [(i, i ^ 1) for i in range(count)])
    block = jnp.concatenate([block, partner], axis=0)
    outer = count // 2
    ahead = [(i, (i // 2 + 1) % outer * 2 + i % 2) for i in range(count)]
    behind = [(i, (i // 2 - 1) % outer * 2 + i % 2) for i in range(count)]
    pieces = [block]
    right, left = block, block
    for _ in range((outer - 1) // 2):
        right = lax.ppermute(right, "ep", ahead)
        left = lax.ppermute(left, "ep", behind)
        pieces += [right, left]
    if outer % 2 == 0:
        pieces.append(lax.ppermute(right[:rows], "ep", ahead))
        pieces.append(lax.ppermute(left[rows:], "ep", behind))
    return pieces


def attention_kernel(piece_count, head_dim, chunk, q_ref, *refs):
    pieces = refs[:piece_count]
    out_ref, wide_values = refs[piece_count], refs[piece_count + 1]
    queries = q_ref[...]
    total = jnp.zeros((queries.shape[0], 2 * head_dim), jnp.float32)
    base = 0
    first = (pl.program_id(0) == 0) & (pl.program_id(1) == 0)

    @pl.when(first)
    def _():
        at = 0
        for piece in pieces:
            rows = piece.shape[0]
            wide_values[at : at + rows, :head_dim] = piece[:, head_dim:]
            wide_values[at : at + rows, head_dim:] = jnp.ones((rows, head_dim), jnp.bfloat16)
            at += rows

    for piece in pieces:
        rows = piece.shape[0]
        step = math.gcd(rows, chunk)
        for start in range(0, rows, step):
            scores = lax.dot_general(
                queries,
                piece[start : start + step, :head_dim],
                (((1,), (1,)), ((), ())),
                preferred_element_type=jnp.float32,
            )
            weights = jnp.exp2(scores).astype(jnp.bfloat16)
            total = total + jnp.dot(
                weights,
                wide_values[base + start : base + start + step, :],
                preferred_element_type=jnp.float32,
            )
        base += rows
    out_ref[...] = (total[:, :head_dim] / total[:, head_dim:]).astype(jnp.bfloat16)


def attend(queries, pieces, head_dim):
    row_count, width = queries.shape
    heads = width // head_dim
    tile = math.gcd(row_count, 256)
    key_count = sum(piece.shape[0] for piece in pieces)
    spec = pl.BlockSpec((tile, head_dim), lambda h, r: (r, h))
    return pl.pallas_call(
        functools.partial(attention_kernel, len(pieces), head_dim, 512),
        out_shape=jax.ShapeDtypeStruct((row_count, width), jnp.bfloat16),
        grid=(heads, row_count // tile),
        in_specs=[spec] + [VMEM] * len(pieces),
        out_specs=spec,
        scratch_shapes=[pltpu.VMEM((key_count, 2 * head_dim), jnp.bfloat16)],
        cost_estimate=pl.CostEstimate(
            flops=8 * row_count * width * key_count,
            bytes_accessed=4 * row_count * width + 4 * key_count * head_dim,
            transcendentals=heads * row_count * key_count,
        ),
        name="attend",
    )(queries, *pieces)


def attention_inputs(queries, keys, values, query_gain, key_gain):
    row_count = queries.shape[0]
    head_dim = query_gain.shape[0]
    heads = queries.shape[1] // head_dim
    assert keys.shape[1] == head_dim
    cos_table, sin_table = rope_angles(row_count, lax.axis_index("ep") * row_count, head_dim)
    krot = norm_rotate(keys.astype(jnp.float32), key_gain, cos_table, sin_table)
    block = jnp.concatenate([krot.astype(jnp.bfloat16), values], axis=1)
    factor = head_dim ** (-0.5) * math.log2(math.e)
    wide = queries.astype(jnp.float32)
    turned = [
        norm_rotate(wide[:, h * head_dim : (h + 1) * head_dim], query_gain, cos_table, sin_table)
        for h in range(heads)
    ]
    return (jnp.concatenate(turned, axis=1) * factor).astype(jnp.bfloat16), block


def project(attended, out_proj):
    tp_count = lax.axis_size("tp")
    row_count, width = attended.shape
    part = row_count // tp_count
    arrived = lax.all_to_all(
        attended.reshape(tp_count, part, width), "tp", split_axis=0, concat_axis=0, tiled=True
    )
    own = arrived.transpose(1, 0, 2).reshape(part, tp_count * width)
    return jnp.dot(own, out_proj, preferred_element_type=jnp.float32).astype(jnp.bfloat16)


def slot_matrix(slot_row, slot_count):
    row_count = slot_row.shape[1]
    places = lax.broadcasted_iota(jnp.int32, (slot_count, row_count), 0)
    return jnp.where(places == slot_row, 1.0, 0.0).astype(jnp.bfloat16)


def dispatch_kernel(capacity, experts, routes_ref, tokens_ref, gain_ref, sender_ref, slots_ref):
    top_count, row_count = routes_ref.shape
    wide = tokens_ref[...].astype(jnp.float32)
    normed = wide * lax.rsqrt(jnp.mean(wide * wide, axis=-1, keepdims=True) + NORM_EPS)
    normed = (normed * gain_ref[...]).astype(jnp.bfloat16)
    before = lax.broadcasted_iota(jnp.int32, (row_count, row_count), 0)
    before = before < lax.broadcasted_iota(jnp.int32, (row_count, row_count), 1)
    before = jnp.where(before, 1.0, 0.0).astype(jnp.bfloat16)
    names = lax.broadcasted_iota(jnp.int32, (experts, row_count), 0)
    taken = jnp.zeros((experts, 1), jnp.float32)
    chosen = None
    for k in range(top_count):
        route = routes_ref[k : k + 1, :]
        onehot = jnp.where(names == route, 1.0, 0.0)
        ahead = jnp.dot(
            onehot.astype(jnp.bfloat16), before, preferred_element_type=jnp.float32
        )
        rank = jnp.sum((ahead + taken) * onehot, axis=0, keepdims=True)
        taken = taken + jnp.sum(onehot, axis=1, keepdims=True)
        slot = route * capacity + rank.astype(jnp.int32)
        slots_ref[k : k + 1, :] = slot
        part = slot_matrix(slot, experts * capacity)
        chosen = part if chosen is None else chosen + part
    sender_ref[...] = jnp.dot(chosen, normed, preferred_element_type=jnp.float32).astype(
        jnp.bfloat16
    )


def combine_kernel(slots_ref, prob_ref, logits_ref, returned_ref, out_ref):
    top_count = slots_ref.shape[0]
    slot_count = returned_ref.shape[0]
    logits = logits_ref[...]
    raised = jnp.exp(logits - jnp.max(logits, axis=1, keepdims=True))
    share = prob_ref[...] * (raised / jnp.sum(raised, axis=1, keepdims=True))
    total = None
    for k in range(top_count):
        picked = lax.dot_general(
            slot_matrix(slots_ref[k : k + 1, :], slot_count),
            returned_ref[...],
            (((0,), (0,)), ((), ())),
            preferred_element_type=jnp.float32,
        )
        term = picked * share[:, k : k + 1]
        total = term if total is None else total + term
    out_ref[...] = total.astype(jnp.bfloat16)


def expert_kernel(x_ref, gate_ref, up_ref, down_ref, out_ref, total):
    inputs = x_ref[...]
    gate_part = jnp.dot(inputs, gate_ref[...], preferred_element_type=jnp.float32)
    up_part = jnp.dot(inputs, up_ref[...], preferred_element_type=jnp.float32)
    hidden = (gate_part / (1.0 + jnp.exp(-gate_part)) * up_part).astype(jnp.bfloat16)
    part = jnp.dot(hidden, down_ref[...], preferred_element_type=jnp.float32)

    @pl.when(pl.program_id(0) == 0)
    def _():
        total[...] = part

    @pl.when(pl.program_id(0) != 0)
    def _():
        total[...] += part

    @pl.when(pl.program_id(0) == pl.num_programs(0) - 1)
    def _():
        out_ref[...] = total[...].astype(jnp.bfloat16)


def expert_apply(inputs, gate_w, up_w, down_w):
    rows, width = inputs.shape
    hidden = gate_w.shape[1]
    tile = math.gcd(hidden, 256)
    return pl.pallas_call(
        expert_kernel,
        out_shape=jax.ShapeDtypeStruct((rows, width), jnp.bfloat16),
        grid=(hidden // tile,),
        in_specs=[
            VMEM,
            pl.BlockSpec((width, tile), lambda i: (0, i)),
            pl.BlockSpec((width, tile), lambda i: (0, i)),
            pl.BlockSpec((tile, width), lambda i: (i, 0)),
        ],
        out_specs=VMEM,
        scratch_shapes=[pltpu.VMEM((rows, width), jnp.float32)],
        cost_estimate=pl.CostEstimate(
            flops=6 * rows * width * hidden,
            bytes_accessed=6 * width * hidden + 4 * rows * width,
            transcendentals=rows * hidden,
        ),
        name="experts",
    )(inputs, gate_w, up_w, down_w)


def body(
    queries,
    keys,
    values,
    query_gain,
    key_gain,
    out_proj,
    tokens_b,
    norm_gain,
    routes,
    group_prob,
    expert_logits,
    w_gate,
    w_up,
    w_down,
):
    device_count = lax.axis_size("ep") * lax.axis_size("tp")
    row_count, top_count = routes.shape
    model_width = tokens_b.shape[1]
    capacity = 2 * top_count * row_count // device_count
    head_dim = query_gain.shape[0]

    queries_in, block = attention_inputs(queries, keys, values, query_gain, key_gain)
    sender, slots = pl.pallas_call(
        functools.partial(dispatch_kernel, capacity, device_count),
        out_shape=(
            jax.ShapeDtypeStruct((device_count * capacity, model_width), jnp.bfloat16),
            jax.ShapeDtypeStruct((top_count, row_count), jnp.int32),
        ),
        in_specs=[VMEM] * 3,
        out_specs=(VMEM, VMEM),
        name="dispatch",
    )(routes.T, tokens_b, norm_gain.reshape(1, model_width))

    def exchange(rows):
        return lax.all_to_all(
            rows.reshape(device_count, capacity, model_width),
            ("ep", "tp"),
            split_axis=0,
            concat_axis=0,
            tiled=True,
        ).reshape(device_count * capacity, model_width)

    pieces = gather_pieces(block)
    arrived = exchange(sender)
    expert_out = expert_apply(arrived, w_gate[0], w_up[0], w_down[0])
    returned = exchange(expert_out)
    attended = attend(queries_in, pieces, head_dim)
    mixed_a = project(attended, out_proj)
    mixed_b = pl.pallas_call(
        combine_kernel,
        out_shape=jax.ShapeDtypeStruct((row_count, model_width), jnp.bfloat16),
        in_specs=[VMEM] * 4,
        out_specs=VMEM,
        name="combine",
    )(slots, group_prob.reshape(row_count, 1), expert_logits, returned)
    return (mixed_a, mixed_b)


def solution(mesh):
    placed = (
        P("ep", "tp"),
        P("ep", "tp"),
        P("ep", "tp"),
        P(),
        P(),
        P(),
        P(("ep", "tp"), None),
        P(),
        P(("ep", "tp"), None),
        P(("ep", "tp")),
        P(("ep", "tp"), None),
        P(("ep", "tp"), None, None),
        P(("ep", "tp"), None, None),
        P(("ep", "tp"), None, None),
    )
    return jax.shard_map(
        body,
        mesh=mesh,
        in_specs=placed,
        out_specs=(P(("ep", "tp"), None), P(("ep", "tp"), None)),
        check_vma=False,
    )
```

time: 215 us -> 177 us (0.82)
  starting transfers between devices: 11.5 us -> 43.4 us
  matrix products: 35.1 us -> 3.73 us
  waiting for transfers between devices: 125 us -> 95.4 us
  Pallas kernels: 0 us -> 23.9 us
  local copies, waits for them, and re-layouts: 18.9 us -> 5.35 us
  between operations: 14 us -> 0.89 us
  other arithmetic: 9.72 us -> 3.75 us
    all_gather x2 -> x0, waiting for transfers between devices: 79.8 us -> none  [the longest x1 40.1 us: attention_half(): value_piece = lax.all_gather(values, 'ep', axis=0, tiled=True)]
    ppermute x0 -> x5, waiting for transfers between devices: none -> 51.9 us  [the longest x1 22.2 us: gather_pieces(): right = lax.ppermute(right, 'ep', ahead)]
    dot_general x11 -> x1, matrix products: 35.1 us -> 3.73 us  [project(): jnp.dot(own, out_proj, preferred_element_type=jnp.float32)]
    ppermute x0 -> x5, starting transfers between devices: none -> 27.1 us  [the longest x1 20.1 us: gather_pieces(): pieces.append(lax.ppermute(right[:rows], 'ep', ahead))]
    pallas_call x0 -> x4, Pallas kernels: none -> 23.9 us  [the longest x1 8.72 us: expert_apply(): pl.pallas_call(expert_kernel, out_shape=jax.ShapeDtypeStruct((rows, width...]
    scatter x1 -> x0, local copies, waits for them, and re-layouts: 7 us -> none  [expert_half(): sender = jnp.zeros((device_count * capacity, model_width), jnp.bfloat16)....]
    reduce_sum x4 -> x0, other arithmetic: 5.89 us -> none  [the longest x1 5.59 us: expert_half(): return jnp.sum(picked * combine[:, :, None], axis=1).astype(jnp.bfloat16)]
    all_to_all x2 -> x3, starting transfers between devices: 11.1 us -> 16.3 us  [the longest x2 12.9 us: exchange(): lax.all_to_all(rows.reshape(device_count, capacity, model_width), ('ep',...]
  transfers between devices with their start and end apart: 5 -> 8, of which waited for: 3 -> 5; matrix products, arithmetic and copies ran while one was open for 23% -> 6% of each run, Pallas kernels for 0% -> 10%
where the time goes in v1:
time: 177 us; the launch traced here: 176 us
  waiting for transfers between devices  95.4 us (54%)
  starting transfers between devices  43.4 us (25%)
  Pallas kernels  23.9 us (14%)
  local copies, waits for them, and re-layouts  5.35 us (3%)
  other arithmetic  3.75 us (2%)
  matrix products  3.73 us (2%)
    all_to_all x2, waiting for transfers between devices, exchange(): lax.all_to_all(rows.reshape(device_count, capacity, model_width), ('ep',...  43.5 us
    ppermute x1, waiting for transfers between devices, gather_pieces(): right = lax.ppermute(right, 'ep', ahead)  22.2 us
    ppermute x1, starting transfers between devices, gather_pieces(): pieces.append(lax.ppermute(right[:rows], 'ep', ahead))  20.1 us
    ppermute x1, waiting for transfers between devices, gather_pieces(): partner = lax.ppermute(block, 'ep', [(i, i ^ 1) for i in range(count)])  18.3 us
    all_to_all x2, starting transfers between devices, exchange(): lax.all_to_all(rows.reshape(device_count, capacity, model_width), ('ep',...  12.9 us
    pallas_call x1, Pallas kernels, expert_apply(): pl.pallas_call(expert_kernel, out_shape=jax.ShapeDtypeStruct((rows, width...  8.72 us
    pallas_call x1, Pallas kernels, attend(): pl.pallas_call(functools.partial(attention_kernel, len(pieces), head_dim,...  8.67 us
    ppermute x1, waiting for transfers between devices, gather_pieces(): pieces.append(lax.ppermute(left[rows:], 'ep', behind))  6.51 us
  transfers between devices with their start and end apart: 8, of which 5 were waited for; matrix products, arithmetic and copies ran while one was open for 6% of the time, Pallas kernels for 10%

profile of v1, /device:TPU:0, one launch (start us, length us, event | category | flops | bytes accessed | tf_op | source)
XLA Modules:
  0.0 176.4 jit_solution(16440068299257063467)
XLA Ops:
  0.6 3.3 %dispatch.1 = (bf16[512,2048]{1,0:T(8,128)(2,1)}, s32[2,128]{1,0:T(2,128)}) custom-call(s32[2,128]{1,0:T(2,128)} %bitcast.23, bf16[128,2048]{1,0:T(8,128)(2,1)} %tokens_ref.1, f32[1,2048]{1,0:T(1,128)} %bitcast.22), custom_call_target="tpu_custom_call" | custom-call | tf_op jit(solution)/shard_map/dispatch/pallas_call | solution.py:272
  3.9 0.0 copy-start.5
  3.9 0.0 copy-start.4
  3.9 0.0 copy-start.9
  3.9 7.3 %all-to-all-start.1 = ((bf16[32,16,2048]{2,1,0:T(8,128)(2,1)}), bf16[32,16,2048]{2,1,0:T(8,128)(2,1)S(1)}, u32[]{:S(2)}, u32[]{:S(2)}) async-start(bf16[32,16,2048]{2,1,0:T(8,128)(2,1)} %bitcast.18), calls=%async_computation.1 | async-start | bytes 4194304 | tf_op jit(solution)/shard_map/all_to_all | solution.py:284
  11.2 0.0 copy-start.10
  11.3 0.0 copy-done.5
  11.4 0.0 copy-done.4
  11.4 0.1 fusion.1
  11.5 0.2 multiply_reduce_fusion.1
  11.8 0.0 copy-done.9
  11.8 0.1 fusion.2
  11.9 0.2 broadcast_multiply_fusion.1
  12.1 0.0 copy-done.10
  12.1 0.2 multiply_multiply_fusion.1
  12.3 0.0 copy-start.2
  12.3 1.2 subtract_convert_fusion
  13.5 0.3 multiply_subtract_fusion.1
  13.9 0.0 copy-done.2
  13.9 0.1 pad_maximum_fusion.2
  14.0 1.8 %collective-permute-start = (bf16[512,256]{1,0:T(8,128)(2,1)S(1)}, bf16[512,256]{1,0:T(8,128)(2,1)S(1)}, u32[]{:S(2)}, u32[]{:S(2)}) collective-permute-start(bf16[512,256]{1,0:T(8,128)(2,1)S(1)} %pad_maximum_fusion.2), channel_id=1, source_target_pairs={{0,4},{4,0},{8,12},{12,8},{16,20},{20,16},{24,28},{28,24},{1,5},{5... | collective-permute-start | bytes 786440 | tf_op jit(solution)/shard_map/ppermute | solution.py:47
  15.9 18.3 %collective-permute-done = bf16[512,256]{1,0:T(8,128)(2,1)S(1)} collective-permute-done((bf16[512,256]{1,0:T(8,128)(2,1)S(1)}, bf16[512,256]{1,0:T(8,128)(2,1)S(1)}, u32[]{:S(2)}, u32[]{:S(2)}) %collective-permute-start) | collective-permute-done | bytes 262176 | tf_op jit(solution)/shard_map/ppermute | solution.py:47
  34.1 0.1 pad_maximum_fusion.refs_0_
  34.3 0.0 copy-start.3
  34.3 0.1 collective-permute-start.1
  34.3 5.0 %collective-permute-start.2 = (bf16[1024,256]{1,0:T(8,128)(2,1)S(1)}, bf16[1024,256]{1,0:T(8,128)(2,1)S(1)}, u32[]{:S(2)}, u32[]{:S(2)}) collective-permute-start(bf16[1024,256]{1,0:T(8,128)(2,1)S(1)} %pad_maximum_fusion.refs_0_), channel_id=1, source_target_pairs={{0,24},{4,28},{8,0},{12,4},{16,8},{20,12},{24,16},{28,20},{1,25},{... | collective-permute-start | bytes 1572872 | tf_op jit(solution)/shard_map/ppermute | solution.py:56
  39.3 22.2 %collective-permute-done.1.refs_1_ = bf16[1024,256]{1,0:T(8,128)(2,1)S(1)} collective-permute-done((bf16[1024,256]{1,0:T(8,128)(2,1)S(1)}, bf16[1024,256]{1,0:T(8,128)(2,1)S(1)}, u32[]{:S(2)}, u32[]{:S(2)}) %collective-permute-start.1) | collective-permute-done | bytes 524320 | tf_op jit(solution)/shard_map/ppermute | solution.py:55
  61.5 0.0 copy-start.6
  61.6 20.1 %collective-permute-start.3 = (bf16[512,256]{1,0:T(8,128)(2,1)S(1)}, bf16[512,256]{1,0:T(8,128)(2,1)S(1)}, u32[]{:S(2)}, u32[]{:S(2)}) collective-permute-start(bf16[512,256]{1,0:T(8,128)(2,1)S(1)} %slice.48), channel_id=1, source_target_pairs={{0,8},{4,12},{8,16},{12,20},{16,24},{20,28},{24,0},{28,4},{1,9},{5... | collective-permute-start | bytes 786440 | tf_op jit(solution)/shard_map/ppermute | solution.py:59
  81.7 0.0 collective-permute-done.2.refs_2_
  81.7 0.0 copy-start.7
  81.7 0.1 collective-permute-start.4
  81.8 0.7 copy-done.7
  82.5 1.0 fusion.q_ref
  83.5 4.9 %collective-permute-done.3.refs_3_ = bf16[512,256]{1,0:T(8,128)(2,1)S(1)} collective-permute-done((bf16[512,256]{1,0:T(8,128)(2,1)S(1)}, bf16[512,256]{1,0:T(8,128)(2,1)S(1)}, u32[]{:S(2)}, u32[]{:S(2)}) %collective-permute-start.3) | collective-permute-done | bytes 262176 | tf_op jit(solution)/shard_map/ppermute | solution.py:59
  88.4 0.0 copy-start.12
  88.4 6.5 %collective-permute-done.4.refs_4_ = bf16[512,256]{1,0:T(8,128)(2,1)} collective-permute-done((bf16[512,256]{1,0:T(8,128)(2,1)S(1)}, bf16[512,256]{1,0:T(8,128)(2,1)}, u32[]{:S(2)}, u32[]{:S(2)}) %collective-permute-start.4) | collective-permute-done | bytes 262176 | tf_op jit(solution)/shard_map/ppermute | solution.py:60
  94.9 0.0 copy-done.3
  94.9 0.0 copy-done.6
  94.9 0.0 copy-done.12
  94.9 8.7 %attend.1 = bf16[512,256]{1,0:T(8,128)(2,1)} custom-call(bf16[512,256]{1,0:T(8,128)(2,1)} %fusion.q_ref, bf16[1024,256]{1,0:T(8,128)(2,1)} %copy-done.3, bf16[1024,256]{1,0:T(8,128)(2,1)} %copy-done.6, bf16[1024,256]{1,0:T(8,128)(2,1)} %copy-done.7, bf16[512,256]{1,0:T(8,128)(2,1)} %copy-done.12, bf16[512,256]{1,0:T(8,128)(2,1)} %collective-permute-done.4.refs_4_), custom_call_target="tpu_custom_call" | custom-call | flops 4294967296 | bytes 2621440 | tf_op jit(solution)/shard_map/attend/pallas_call | solution.py:107
  103.6 1.8 %copy.18 = bf16[4,128,256]{1,2,0:T(8,128)(2,1)} copy(bf16[4,128,256]{2,1,0:T(8,128)(2,1)} %bitcast.21) | data formatting | bytes 524288 | tf_op jit(solution)/shard_map/reshape | solution.py:145
  105.4 0.0 all-to-all-done.1
  105.4 0.0 copy-start.1
  105.4 3.4 %all-to-all-start = ((bf16[4,128,256]{1,2,0:T(8,128)(2,1)}), bf16[4,128,256]{1,2,0:T(8,128)(2,1)S(1)}, u32[]{:S(2)}, u32[]{:S(2)}) async-start(bf16[4,128,256]{1,2,0:T(8,128)(2,1)} %copy.18), calls=%async_computation | async-start | bytes 524288 | tf_op jit(solution)/shard_map/all_to_all | solution.py:144
  108.8 0.0 copy-done.1
  108.8 8.7 %experts.1 = bf16[512,2048]{1,0:T(8,128)(2,1)} custom-call(bf16[512,2048]{1,0:T(8,128)(2,1)} %bitcast.17, bf16[2048,512]{1,0:T(8,128)(2,1)} %bitcast.25, bf16[2048,512]{1,0:T(8,128)(2,1)} %bitcast.26, bf16[512,2048]{1,0:T(8,128)(2,1)} %bitcast.27), custom_call_target="tpu_custom_call" | custom-call | flops 3221225472 | bytes 10485760 | tf_op jit(solution)/shard_map/experts/pallas_call | solution.py:228
  117.5 0.0 all-to-all-done
  117.5 0.0 copy-start.11
  117.5 0.0 copy-start.8
  117.6 5.5 %all-to-all-start.2 = ((bf16[32,16,2048]{2,1,0:T(8,128)(2,1)}), bf16[32,16,2048]{2,1,0:T(8,128)(2,1)S(1)}, u32[]{:S(2)}, u32[]{:S(2)}) async-start(bf16[32,16,2048]{2,1,0:T(8,128)(2,1)} %bitcast.19), calls=%async_computation.2 | async-start | bytes 4194304 | tf_op jit(solution)/shard_map/all_to_all | solution.py:284
  123.1 0.0 copy-done.11
  123.1 0.7 copy.19.prob_ref
  123.8 0.0 copy-done.8
  123.8 0.7 copy.20.logits_ref
  124.6 3.7 %convolution_convert_fusion = bf16[128,2048]{1,0:T(8,128)(2,1)} fusion(bf16[128,1024]{0,1:T(8,128)(2,1)S(1)} %bitcast.20, bf16[1024,2048]{1,0:T(8,128)(2,1)} %param.19), kind=kOutput, calls=%fused_computation | convolution fusion | flops 537133056 | bytes 4980736 | tf_op jit(solution)/shard_map/dot_general | solution.py:148
  128.3 43.5 %all-to-all-done.2 = bf16[32,16,2048]{2,1,0:T(8,128)(2,1)S(1)} async-done(((bf16[32,16,2048]{2,1,0:T(8,128)(2,1)}), bf16[32,16,2048]{2,1,0:T(8,128)(2,1)S(1)}, u32[]{:S(2)}, u32[]{:S(2)}) %all-to-all-start.2) | async-done | bytes 2097184 | tf_op jit(solution)/shard_map/all_to_all | solution.py:284
  171.8 0.0 copy-start
  171.8 1.3 copy-done
  173.1 3.2 %combine.1 = bf16[128,2048]{1,0:T(8,128)(2,1)} custom-call(s32[2,128]{1,0:T(2,128)} %get-tuple-element.4.slots_ref, f32[128,1]{1,0:T(8,128)} %copy.19.prob_ref, f32[128,2]{1,0:T(8,128)} %copy.20.logits_ref, bf16[512,2048]{1,0:T(8,128)(2,1)} %bitcast.16), custom_call_target="tpu_custom_call" | custom-call | tf_op jit(solution)/shard_map/combine/pallas_call | solution.py:298
  (7 shorter events, 0.1 us)
Async XLA Ops:
  3.9 7.4 %copy-start.5 = (bf16[512,256]{1,0:T(8,128)(2,1)S(1)}, bf16[512,256]{1,0:T(8,128)(2,1)}, u32[]{:S(2)}) copy-start(bf16[512,256]{1,0:T(8,128)(2,1)} %param.14) | copy-start | bytes 786436
  3.9 7.5 %copy-start.4 = (bf16[512,128]{1,0:T(8,128)(2,1)S(1)}, bf16[512,128]{1,0:T(8,128)(2,1)}, u32[]{:S(2)}) copy-start(bf16[512,128]{1,0:T(8,128)(2,1)} %param.15) | copy-start | bytes 393220
  3.9 7.9 %copy-start.9 = (f32[128]{0:T(128)S(1)}, f32[128]{0:T(128)}, u32[]{:S(2)}) copy-start(f32[128]{0:T(128)} %param.18) | copy-start | bytes 1540
  3.9 101.5 %all-to-all-start.1 = ((bf16[32,16,2048]{2,1,0:T(8,128)(2,1)}), bf16[32,16,2048]{2,1,0:T(8,128)(2,1)S(1)}, u32[]{:S(2)}, u32[]{:S(2)}) async-start(bf16[32,16,2048]{2,1,0:T(8,128)(2,1)} %bitcast.18), calls=%async_computation.1 | async-start | bytes 4194304 | tf_op jit(solution)/shard_map/all_to_all | solution.py:284
  11.2 0.9 copy-start.10
  12.3 1.5 copy-start.2
  14.0 20.1 %collective-permute-start = (bf16[512,256]{1,0:T(8,128)(2,1)S(1)}, bf16[512,256]{1,0:T(8,128)(2,1)S(1)}, u32[]{:S(2)}, u32[]{:S(2)}) collective-permute-start(bf16[512,256]{1,0:T(8,128)(2,1)S(1)} %pad_maximum_fusion.2), channel_id=1, source_target_pairs={{0,4},{4,0},{8,12},{12,8},{16,20},{20,16},{24,28},{28,24},{1,5},{5... | collective-permute-start | bytes 786440 | tf_op jit(solution)/shard_map/ppermute | solution.py:47
  34.3 60.6 %copy-start.3 = (bf16[1024,256]{1,0:T(8,128)(2,1)}, bf16[1024,256]{1,0:T(8,128)(2,1)S(1)}, u32[]{:S(2)}) copy-start(bf16[1024,256]{1,0:T(8,128)(2,1)S(1)} %pad_maximum_fusion.refs_0_) | copy-start | bytes 1572868
  34.3 27.3 %collective-permute-start.1 = (bf16[1024,256]{1,0:T(8,128)(2,1)S(1)}, bf16[1024,256]{1,0:T(8,128)(2,1)S(1)}, u32[]{:S(2)}, u32[]{:S(2)}) collective-permute-start(bf16[1024,256]{1,0:T(8,128)(2,1)S(1)} %pad_maximum_fusion.refs_0_), channel_id=1, source_target_pairs={{0,8},{4,12},{8,16},{12,20},{16,24},{20,28},{24,0},{28,4},{1,9},{5... | collective-permute-start | bytes 1572872 | tf_op jit(solution)/shard_map/ppermute | solution.py:55
  34.3 47.4 %collective-permute-start.2 = (bf16[1024,256]{1,0:T(8,128)(2,1)S(1)}, bf16[1024,256]{1,0:T(8,128)(2,1)S(1)}, u32[]{:S(2)}, u32[]{:S(2)}) collective-permute-start(bf16[1024,256]{1,0:T(8,128)(2,1)S(1)} %pad_maximum_fusion.refs_0_), channel_id=1, source_target_pairs={{0,24},{4,28},{8,0},{12,4},{16,8},{20,12},{24,16},{28,20},{1,25},{... | collective-permute-start | bytes 1572872 | tf_op jit(solution)/shard_map/ppermute | solution.py:56
  61.5 33.4 %copy-start.6 = (bf16[1024,256]{1,0:T(8,128)(2,1)}, bf16[1024,256]{1,0:T(8,128)(2,1)S(1)}, u32[]{:S(2)}) copy-start(bf16[1024,256]{1,0:T(8,128)(2,1)S(1)} %collective-permute-done.1.refs_1_) | copy-start | bytes 1572868
  61.6 26.8 %collective-permute-start.3 = (bf16[512,256]{1,0:T(8,128)(2,1)S(1)}, bf16[512,256]{1,0:T(8,128)(2,1)S(1)}, u32[]{:S(2)}, u32[]{:S(2)}) collective-permute-start(bf16[512,256]{1,0:T(8,128)(2,1)S(1)} %slice.48), channel_id=1, source_target_pairs={{0,8},{4,12},{8,16},{12,20},{16,24},{20,28},{24,0},{28,4},{1,9},{5... | collective-permute-start | bytes 786440 | tf_op jit(solution)/shard_map/ppermute | solution.py:59
  81.7 0.8 copy-start.7
  81.7 13.2 %collective-permute-start.4 = (bf16[512,256]{1,0:T(8,128)(2,1)S(1)}, bf16[512,256]{1,0:T(8,128)(2,1)}, u32[]{:S(2)}, u32[]{:S(2)}) collective-permute-start(bf16[512,256]{1,0:T(8,128)(2,1)S(1)} %slice.49), channel_id=1, source_target_pairs={{0,24},{4,28},{8,0},{12,4},{16,8},{20,12},{24,16},{28,20},{1,25},{... | collective-permute-start | bytes 786440 | tf_op jit(solution)/shard_map/ppermute | solution.py:60
  88.4 6.5 %copy-start.12 = (bf16[512,256]{1,0:T(8,128)(2,1)}, bf16[512,256]{1,0:T(8,128)(2,1)S(1)}, u32[]{:S(2)}) copy-start(bf16[512,256]{1,0:T(8,128)(2,1)S(1)} %collective-permute-done.3.refs_3_) | copy-start | bytes 786436
  105.4 3.4 %copy-start.1 = (bf16[32,16,2048]{2,1,0:T(8,128)(2,1)}, bf16[32,16,2048]{2,1,0:T(8,128)(2,1)S(1)}, u32[]{:S(2)}) copy-start(bf16[32,16,2048]{2,1,0:T(8,128)(2,1)S(1)} %all-to-all-done.1) | copy-start | bytes 6291460
  105.4 12.2 %all-to-all-start = ((bf16[4,128,256]{1,2,0:T(8,128)(2,1)}), bf16[4,128,256]{1,2,0:T(8,128)(2,1)S(1)}, u32[]{:S(2)}, u32[]{:S(2)}) async-start(bf16[4,128,256]{1,2,0:T(8,128)(2,1)} %copy.18), calls=%async_computation | async-start | bytes 524288 | tf_op jit(solution)/shard_map/all_to_all | solution.py:144
  117.5 5.5 %copy-start.11 = (f32[128]{0:T(128)S(1)}, f32[128]{0:T(128)}, u32[]{:S(2)}) copy-start(f32[128]{0:T(128)} %param.23) | copy-start | bytes 1540
  117.5 6.3 %copy-start.8 = (f32[128,2]{0,1:T(2,128)S(1)}, f32[128,2]{0,1:T(2,128)}, u32[]{:S(2)}) copy-start(f32[128,2]{0,1:T(2,128)} %param.24) | copy-start | bytes 3076
  117.6 54.3 %all-to-all-start.2 = ((bf16[32,16,2048]{2,1,0:T(8,128)(2,1)}), bf16[32,16,2048]{2,1,0:T(8,128)(2,1)S(1)}, u32[]{:S(2)}, u32[]{:S(2)}) async-start(bf16[32,16,2048]{2,1,0:T(8,128)(2,1)} %bitcast.19), calls=%async_computation.2 | async-start | bytes 4194304 | tf_op jit(solution)/shard_map/all_to_all | solution.py:284
  171.8 1.3 copy-start

commit v2 on v1

--- a/solution.py
+++ b/solution.py
@@ -39,14 +39,31 @@
     )
 
 
-def gather_pieces(block):
+def gather_pieces(block, gate):
     count = lax.axis_size("ep")
     rows = block.shape[0]
     if count % 2 or count < 4:
-        return [lax.all_gather(block, "ep", axis=0, tiled=True)]
-    partner = lax.ppermute(block, "ep", [(i, i ^ 1) for i in range(count)])
+        return [lax.all_gather(block, "ep", axis=0, tiled=True)], gate
+    outer = count // 2
+    swap = [(i, i ^ 1) for i in range(count)]
+    if outer <= 4:
+        ahead = [(i, i + 2) for i in range(count - 2)]
+        behind = [(i + 2, i) for i in range(count - 2)]
+        rights, lefts = [block], [block]
+        pieces = [block, lax.ppermute(block, "ep", swap)]
+        for step in range(1, outer):
+            rights.append(lax.ppermute(rights[-1], "ep", ahead))
+            lefts.append(lax.ppermute(lefts[-1], "ep", behind))
+            if step == 1:
+                gate, rights[1], lefts[1], pieces[1] = lax.optimization_barrier(
+                    (gate, rights[1], lefts[1], pieces[1])
+                )
+        for step in range(1, outer):
+            piece = rights[step] + lefts[outer - step]
+            pieces += [piece, lax.ppermute(piece, "ep", swap)]
+        return pieces, gate
+    partner = lax.ppermute(block, "ep", swap)
     block = jnp.concatenate([block, partner], axis=0)
-    outer = count // 2
     ahead = [(i, (i // 2 + 1) % outer * 2 + i % 2) for i in range(count)]
     behind = [(i, (i // 2 - 1) % outer * 2 + i % 2) for i in range(count)]
     pieces = [block]
@@ -58,7 +75,7 @@
     if outer % 2 == 0:
         pieces.append(lax.ppermute(right[:rows], "ep", ahead))
         pieces.append(lax.ppermute(left[rows:], "ep", behind))
-    return pieces
+    return pieces, gate
 
 
 def attention_kernel(piece_count, head_dim, chunk, q_ref, *refs):
@@ -289,9 +306,10 @@
             tiled=True,
         ).reshape(device_count * capacity, model_width)
 
-    pieces = gather_pieces(block)
+    pieces, sender = gather_pieces(block, sender)
     arrived = exchange(sender)
     expert_out = expert_apply(arrived, w_gate[0], w_up[0], w_down[0])
+    queries_in, expert_out = lax.optimization_barrier((queries_in, expert_out))
     returned = exchange(expert_out)
     attended = attend(queries_in, pieces, head_dim)
     mixed_a = project(attended, out_proj)

time: 177 us -> 183 us (1.034)
  waiting for transfers between devices: 95.4 us -> 85 us
  blocking collectives: 0 us -> 8.66 us
  other arithmetic: 3.75 us -> 6.56 us
  starting transfers between devices: 43.4 us -> 46.2 us
    ppermute x5 -> x10, waiting for transfers between devices: 51.9 us -> 41.4 us  [the longest x3 34.9 us: gather_pieces(): lefts.append(lax.ppermute(lefts[-1], 'ep', behind))]
    ppermute x5 -> x10, starting transfers between devices: 27.1 us -> 37.2 us  [the longest x3 27.5 us: gather_pieces(): rights.append(lax.ppermute(rights[-1], 'ep', ahead))]
    all_to_all x0 -> x1, blocking collectives: none -> 8.66 us  [project(): lax.all_to_all(attended.reshape(tp_count, part, width), 'tp', split_axis=...]
    all_to_all x2, starting transfers between devices: 12.9 us -> 9.04 us  [exchange(): lax.all_to_all(rows.reshape(device_count, capacity, model_width), ('ep',...]
    all_to_all x1 -> x0, starting transfers between devices: 3.41 us -> none  [project(): lax.all_to_all(attended.reshape(tp_count, part, width), 'tp', split_axis=...]
    unnamed x27 -> x31, local copies, waits for them, and re-layouts: 2.8 us -> 5.19 us
  transfers between devices with their start and end apart: 8 -> 12, of which waited for: 5 -> 6; matrix products, arithmetic and copies ran while one was open for 6% -> 4% of each run, Pallas kernels for 10% -> 7%
where the time goes in v2:
time: 183 us; the launch traced here: 182 us
  waiting for transfers between devices  85 us (46%)
  starting transfers between devices  46.2 us (25%)
  Pallas kernels  23.9 us (13%)
  blocking collectives  8.66 us (5%)
  local copies, waits for them, and re-layouts  7.05 us (4%)
  other arithmetic  6.56 us (4%)
  matrix products  3.73 us (2%)
    all_to_all x2, waiting for transfers between devices, exchange(): lax.all_to_all(rows.reshape(device_count, capacity, model_width), ('ep',...  43.5 us
    ppermute x3, waiting for transfers between devices, gather_pieces(): lefts.append(lax.ppermute(lefts[-1], 'ep', behind))  34.9 us
    ppermute x3, starting transfers between devices, gather_pieces(): rights.append(lax.ppermute(rights[-1], 'ep', ahead))  27.5 us
    all_to_all x2, starting transfers between devices, exchange(): lax.all_to_all(rows.reshape(device_count, capacity, model_width), ('ep',...  9.04 us
    pallas_call x1, Pallas kernels, expert_apply(): pl.pallas_call(expert_kernel, out_shape=jax.ShapeDtypeStruct((rows, width...  8.72 us
    pallas_call x1, Pallas kernels, attend(): pl.pallas_call(functools.partial(attention_kernel, len(pieces), head_dim,...  8.67 us
    all_to_all x1, blocking collectives, project(): lax.all_to_all(attended.reshape(tp_count, part, width), 'tp', split_axis=...  8.66 us
    unnamed x31, local copies, waits for them, and re-layouts  5.19 us
  transfers between devices with their start and end apart: 12, of which 6 were waited for; matrix products, arithmetic and copies ran while one was open for 4% of the time, Pallas kernels for 7%

profile of v2, /device:TPU:0, one launch (start us, length us, event | category | flops | bytes accessed | tf_op | source)
XLA Modules:
  0.0 182.0 jit_solution(7785279959857388691)
XLA Ops:
  0.6 0.0 copy-start.10
  0.7 1.1 fusion.1
  1.7 1.0 convert_element_type.27
  2.7 0.2 multiply_reduce_fusion.1
  3.0 1.0 fusion.2
  4.0 0.2 broadcast_multiply_fusion.1
  4.2 1.2 subtract_convert_fusion
  5.4 0.0 copy-done.10
  5.4 0.0 copy-start.8
  5.4 0.2 multiply_multiply_fusion.1
  5.6 0.3 multiply_subtract_fusion.1
  6.0 0.4 copy-done.8
  6.3 0.1 pad_maximum_fusion.1.refs_0_
  6.5 0.0 copy-start.7
  6.5 5.0 %collective-permute-start = (bf16[512,256]{1,0:T(8,128)(2,1)S(1)}, bf16[512,256]{1,0:T(8,128)(2,1)S(1)}, u32[]{:S(2)}, u32[]{:S(2)}) collective-permute-start(bf16[512,256]{1,0:T(8,128)(2,1)S(1)} %pad_maximum_fusion.1.refs_0_), channel_id=1, source_target_pairs={{0,8},{4,12},{8,16},{12,20},{16,24},{20,28},{1,9},{5,13},{9,17},{1... | collective-permute-start | bytes 786440 | tf_op jit(solution)/shard_map/ppermute | solution.py:55
  11.5 1.3 collective-permute-start.1
  12.8 1.6 collective-permute-start.2
  14.4 3.3 %dispatch.1 = (bf16[512,2048]{1,0:T(8,128)(2,1)}, s32[2,128]{1,0:T(2,128)}) custom-call(s32[2,128]{1,0:T(2,128)} %bitcast.23, bf16[128,2048]{1,0:T(8,128)(2,1)} %tokens_ref.1, f32[1,2048]{1,0:T(1,128)} %bitcast.22), custom_call_target="tpu_custom_call" | custom-call | tf_op jit(solution)/shard_map/dispatch/pallas_call | solution.py:289
  17.6 0.0 collective-permute-done
  17.6 3.5 %collective-permute-done.1 = bf16[512,256]{1,0:T(8,128)(2,1)S(1)} collective-permute-done((bf16[512,256]{1,0:T(8,128)(2,1)S(1)}, bf16[512,256]{1,0:T(8,128)(2,1)S(1)}, u32[]{:S(2)}, u32[]{:S(2)}) %collective-permute-start.1) | collective-permute-done | bytes 262176 | tf_op jit(solution)/shard_map/ppermute | solution.py:56
  21.1 0.0 collective-permute-done.2.refs_1_
  21.1 0.0 copy-done.7
  21.1 0.0 copy-done.2
  21.2 0.7 copy-done.12
  21.8 6.1 %all-to-all-start = ((bf16[32,16,2048]{2,1,0:T(8,128)(2,1)}), bf16[32,16,2048]{2,1,0:T(8,128)(2,1)S(1)}, u32[]{:S(2)}, u32[]{:S(2)}) async-start(bf16[32,16,2048]{2,1,0:T(8,128)(2,1)} %bitcast.17), calls=%async_computation | async-start | bytes 4194304 | tf_op jit(solution)/shard_map/all_to_all | solution.py:301
  28.0 0.0 copy-start.3
  28.0 1.4 collective-permute-start.3
  29.4 4.6 %collective-permute-start.6 = (bf16[512,256]{1,0:T(8,128)(2,1)}, bf16[512,256]{1,0:T(8,128)(2,1)S(1)}, u32[]{:S(2)}, u32[]{:S(2)}) collective-permute-start(bf16[512,256]{1,0:T(8,128)(2,1)} %copy-done.2), channel_id=1, source_target_pairs={{0,8},{4,12},{8,16},{12,20},{16,24},{20,28},{1,9},{5,13},{9,17},{1... | collective-permute-start | bytes 786440 | tf_op jit(solution)/shard_map/ppermute | solution.py:55
  34.0 29.9 %collective-permute-done.3 = bf16[512,256]{1,0:T(8,128)(2,1)S(1)} collective-permute-done((bf16[512,256]{1,0:T(8,128)(2,1)S(1)}, bf16[512,256]{1,0:T(8,128)(2,1)S(1)}, u32[]{:S(2)}, u32[]{:S(2)}) %collective-permute-start.3) | collective-permute-done | bytes 262176 | tf_op jit(solution)/shard_map/ppermute | solution.py:56
  63.9 1.3 collective-permute-start.4
  65.2 3.6 %collective-permute-done.6 = bf16[512,256]{1,0:T(8,128)(2,1)S(1)} collective-permute-done((bf16[512,256]{1,0:T(8,128)(2,1)}, bf16[512,256]{1,0:T(8,128)(2,1)S(1)}, u32[]{:S(2)}, u32[]{:S(2)}) %collective-permute-start.6) | collective-permute-done | bytes 262176 | tf_op jit(solution)/shard_map/ppermute | solution.py:55
  68.7 18.0 %collective-permute-start.8 = (bf16[512,256]{1,0:T(8,128)(2,1)S(1)}, bf16[512,256]{1,0:T(8,128)(2,1)S(1)}, u32[]{:S(2)}, u32[]{:S(2)}) collective-permute-start(bf16[512,256]{1,0:T(8,128)(2,1)S(1)} %collective-permute-done.6), channel_id=1, source_target_pairs={{0,8},{4,12},{8,16},{12,20},{16,24},{20,28},{1,9},{5,13},{9,17},{1... | collective-permute-start | bytes 786440 | tf_op jit(solution)/shard_map/ppermute | solution.py:55
  86.7 1.0 fusion.q_ref
  87.7 0.1 add.80.refs_4_
  87.8 0.0 copy-start.4
  87.8 1.5 collective-permute-start.7
  89.3 1.5 collective-permute-done.4
  90.8 0.0 copy-done.3
  90.8 0.1 add.79.refs_2_
  90.8 0.0 copy-start.5
  90.8 1.5 collective-permute-start.5
  92.3 0.0 collective-permute-done.8
  92.3 0.1 add.81.refs_6_
  92.4 0.0 copy-start.6
  92.4 1.1 collective-permute-start.9
  93.5 0.0 all-to-all-done
  93.5 1.3 copy-done.1
  94.9 8.7 %experts.1 = bf16[512,2048]{1,0:T(8,128)(2,1)} custom-call(bf16[512,2048]{1,0:T(8,128)(2,1)} %bitcast.18, bf16[2048,512]{1,0:T(8,128)(2,1)} %bitcast.25, bf16[2048,512]{1,0:T(8,128)(2,1)} %bitcast.26, bf16[512,2048]{1,0:T(8,128)(2,1)} %bitcast.27), custom_call_target="tpu_custom_call" | custom-call | flops 3221225472 | bytes 10485760 | tf_op jit(solution)/shard_map/experts/pallas_call | solution.py:245
  103.6 0.0 copy-done.5
  103.6 0.0 collective-permute-done.7.refs_5_
  103.6 0.0 collective-permute-done.5.refs_3_
  103.6 2.9 %collective-permute-done.9.refs_7_ = bf16[512,256]{1,0:T(8,128)(2,1)S(1)} collective-permute-done((bf16[512,256]{1,0:T(8,128)(2,1)S(1)}, bf16[512,256]{1,0:T(8,128)(2,1)S(1)}, u32[]{:S(2)}, u32[]{:S(2)}) %collective-permute-start.9) | collective-permute-done | bytes 262176 | tf_op jit(solution)/shard_map/ppermute | solution.py:63
  106.6 0.7 copy-done.14
  107.3 8.7 %attend.1 = bf16[512,256]{1,0:T(8,128)(2,1)} custom-call(bf16[512,256]{1,0:T(8,128)(2,1)} %fusion.q_ref, bf16[512,256]{1,0:T(8,128)(2,1)} %copy-done.7, bf16[512,256]{1,0:T(8,128)(2,1)} %copy-done.12, bf16[512,256]{1,0:T(8,128)(2,1)} %copy-done.5, bf16[512,256]{1,0:T(8,128)(2,1)} %collective-permute-done.5.refs_3_, bf16[512,256]{1,0:T(8,128)(2,1)} %copy-done.4, ...), custom_call_target="tpu_custom_call" | custom-call | flops 4294967296 | bytes 2621440 | tf_op jit(solution)/shard_map/attend/pallas_call | solution.py:124
  115.9 1.1 copy.18
  117.1 8.7 %all_to_all.15 = bf16[4,128,256]{1,2,0:T(8,128)(2,1)S(1)} all-to-all(bf16[4,128,256]{1,2,0:T(8,128)(2,1)S(1)} %copy.18), channel_id=1, replica_groups=mesh['ep'=8,'tp'=4] {'tp'}, dimensions={0} | all-to-all | bytes 524288 | tf_op jit(solution)/shard_map/all_to_all | solution.py:161
  125.7 2.9 %all-to-all-start.2 = ((bf16[32,16,2048]{2,1,0:T(8,128)(2,1)}), bf16[32,16,2048]{2,1,0:T(8,128)(2,1)S(1)}, u32[]{:S(2)}, u32[]{:S(2)}) async-start(bf16[32,16,2048]{2,1,0:T(8,128)(2,1)} %bitcast.19), calls=%async_computation.2 | async-start | bytes 4194304 | tf_op jit(solution)/shard_map/all_to_all | solution.py:301
  128.7 0.7 copy.19.prob_ref
  129.4 0.0 copy-done.9
  129.4 0.7 copy.20.logits_ref
  130.2 3.7 %convolution_convert_fusion = bf16[128,2048]{1,0:T(8,128)(2,1)} fusion(bf16[128,1024]{0,1:T(8,128)(2,1)S(1)} %bitcast.20, bf16[1024,2048]{1,0:T(8,128)(2,1)} %param.19), kind=kOutput, calls=%fused_computation | convolution fusion | flops 537133056 | bytes 4980736 | tf_op jit(solution)/shard_map/dot_general | solution.py:165
  133.9 43.5 %all-to-all-done.2 = bf16[32,16,2048]{2,1,0:T(8,128)(2,1)S(1)} async-done(((bf16[32,16,2048]{2,1,0:T(8,128)(2,1)}), bf16[32,16,2048]{2,1,0:T(8,128)(2,1)S(1)}, u32[]{:S(2)}, u32[]{:S(2)}) %all-to-all-start.2) | async-done | bytes 2097184 | tf_op jit(solution)/shard_map/all_to_all | solution.py:301
  177.4 1.3 copy-done
  178.7 3.2 %combine.1 = bf16[128,2048]{1,0:T(8,128)(2,1)} custom-call(s32[2,128]{1,0:T(2,128)} %get-tuple-element.16.slots_ref, f32[128,1]{1,0:T(8,128)} %copy.19.prob_ref, f32[128,2]{1,0:T(8,128)} %copy.20.logits_ref, bf16[512,2048]{1,0:T(8,128)(2,1)} %bitcast.16), custom_call_target="tpu_custom_call" | custom-call | tf_op jit(solution)/shard_map/combine/pallas_call | solution.py:316
  (16 shorter events, 0.1 us)
Async XLA Ops:
  0.6 4.8 %copy-start.10 = (f32[128]{0:T(128)S(1)}, f32[128]{0:T(128)}, u32[]{:S(2)}) copy-start(f32[128]{0:T(128)} %param.17) | copy-start | bytes 1540
  5.4 0.9 copy-start.8
  6.5 14.7 %copy-start.7 = (bf16[512,256]{1,0:T(8,128)(2,1)}, bf16[512,256]{1,0:T(8,128)(2,1)S(1)}, u32[]{:S(2)}) copy-start(bf16[512,256]{1,0:T(8,128)(2,1)S(1)} %pad_maximum_fusion.1.refs_0_) | copy-start | bytes 786436
  6.5 11.2 %collective-permute-start = (bf16[512,256]{1,0:T(8,128)(2,1)S(1)}, bf16[512,256]{1,0:T(8,128)(2,1)S(1)}, u32[]{:S(2)}, u32[]{:S(2)}) collective-permute-start(bf16[512,256]{1,0:T(8,128)(2,1)S(1)} %pad_maximum_fusion.1.refs_0_), channel_id=1, source_target_pairs={{0,8},{4,12},{8,16},{12,20},{16,24},{20,28},{1,9},{5,13},{9,17},{1... | collective-permute-start | bytes 786440 | tf_op jit(solution)/shard_map/ppermute | solution.py:55
  11.5 9.7 %collective-permute-start.1 = (bf16[512,256]{1,0:T(8,128)(2,1)S(1)}, bf16[512,256]{1,0:T(8,128)(2,1)S(1)}, u32[]{:S(2)}, u32[]{:S(2)}) collective-permute-start(bf16[512,256]{1,0:T(8,128)(2,1)S(1)} %pad_maximum_fusion.1.refs_0_), channel_id=1, source_target_pairs={{8,0},{12,4},{16,8},{20,12},{24,16},{28,20},{9,1},{13,5},{17,9},{2... | collective-permute-start | bytes 786440 | tf_op jit(solution)/shard_map/ppermute | solution.py:56
  12.8 8.4 %collective-permute-start.2 = (bf16[512,256]{1,0:T(8,128)(2,1)S(1)}, bf16[512,256]{1,0:T(8,128)(2,1)S(1)}, u32[]{:S(2)}, u32[]{:S(2)}) collective-permute-start(bf16[512,256]{1,0:T(8,128)(2,1)S(1)} %pad_maximum_fusion.1.refs_0_), channel_id=1, source_target_pairs={{0,4},{4,0},{8,12},{12,8},{16,20},{20,16},{24,28},{28,24},{1,5},{5... | collective-permute-start | bytes 786440 | tf_op jit(solution)/shard_map/ppermute | solution.py:53
  17.6 3.5 %copy-start.2 = (bf16[512,256]{1,0:T(8,128)(2,1)}, bf16[512,256]{1,0:T(8,128)(2,1)S(1)}, u32[]{:S(2)}) copy-start(bf16[512,256]{1,0:T(8,128)(2,1)S(1)} %collective-permute-done) | copy-start | bytes 786436
  21.1 0.7 copy-start.12
  21.8 71.7 %all-to-all-start = ((bf16[32,16,2048]{2,1,0:T(8,128)(2,1)}), bf16[32,16,2048]{2,1,0:T(8,128)(2,1)S(1)}, u32[]{:S(2)}, u32[]{:S(2)}) async-start(bf16[32,16,2048]{2,1,0:T(8,128)(2,1)} %bitcast.17), calls=%async_computation | async-start | bytes 4194304 | tf_op jit(solution)/shard_map/all_to_all | solution.py:301
  28.0 62.8 %copy-start.3 = (bf16[512,256]{1,0:T(8,128)(2,1)S(1)}, bf16[512,256]{1,0:T(8,128)(2,1)}, u32[]{:S(2)}) copy-start(bf16[512,256]{1,0:T(8,128)(2,1)} %copy-done.2) | copy-start | bytes 786436
  28.0 35.9 %collective-permute-start.3 = (bf16[512,256]{1,0:T(8,128)(2,1)S(1)}, bf16[512,256]{1,0:T(8,128)(2,1)S(1)}, u32[]{:S(2)}, u32[]{:S(2)}) collective-permute-start(bf16[512,256]{1,0:T(8,128)(2,1)S(1)} %collective-permute-done.1), channel_id=1, source_target_pairs={{8,0},{12,4},{16,8},{20,12},{24,16},{28,20},{9,1},{13,5},{17,9},{2... | collective-permute-start | bytes 786440 | tf_op jit(solution)/shard_map/ppermute | solution.py:56
  29.4 39.4 %collective-permute-start.6 = (bf16[512,256]{1,0:T(8,128)(2,1)}, bf16[512,256]{1,0:T(8,128)(2,1)S(1)}, u32[]{:S(2)}, u32[]{:S(2)}) collective-permute-start(bf16[512,256]{1,0:T(8,128)(2,1)} %copy-done.2), channel_id=1, source_target_pairs={{0,8},{4,12},{8,16},{12,20},{16,24},{20,28},{1,9},{5,13},{9,17},{1... | collective-permute-start | bytes 786440 | tf_op jit(solution)/shard_map/ppermute | solution.py:55
  63.9 26.9 %collective-permute-start.4 = (bf16[512,256]{1,0:T(8,128)(2,1)S(1)}, bf16[512,256]{1,0:T(8,128)(2,1)S(1)}, u32[]{:S(2)}, u32[]{:S(2)}) collective-permute-start(bf16[512,256]{1,0:T(8,128)(2,1)S(1)} %collective-permute-done.3), channel_id=1, source_target_pairs={{8,0},{12,4},{16,8},{20,12},{24,16},{28,20},{9,1},{13,5},{17,9},{2... | collective-permute-start | bytes 786440 | tf_op jit(solution)/shard_map/ppermute | solution.py:56
  68.7 23.6 %collective-permute-start.8 = (bf16[512,256]{1,0:T(8,128)(2,1)S(1)}, bf16[512,256]{1,0:T(8,128)(2,1)S(1)}, u32[]{:S(2)}, u32[]{:S(2)}) collective-permute-start(bf16[512,256]{1,0:T(8,128)(2,1)S(1)} %collective-permute-done.6), channel_id=1, source_target_pairs={{0,8},{4,12},{8,16},{12,20},{16,24},{20,28},{1,9},{5,13},{9,17},{1... | collective-permute-start | bytes 786440 | tf_op jit(solution)/shard_map/ppermute | solution.py:55
  87.8 15.8 %copy-start.4 = (bf16[512,256]{1,0:T(8,128)(2,1)}, bf16[512,256]{1,0:T(8,128)(2,1)S(1)}, u32[]{:S(2)}) copy-start(bf16[512,256]{1,0:T(8,128)(2,1)S(1)} %add.80.refs_4_) | copy-start | bytes 786436
  87.8 15.8 %collective-permute-start.7 = (bf16[512,256]{1,0:T(8,128)(2,1)S(1)}, bf16[512,256]{1,0:T(8,128)(2,1)S(1)}, u32[]{:S(2)}, u32[]{:S(2)}) collective-permute-start(bf16[512,256]{1,0:T(8,128)(2,1)S(1)} %add.80.refs_4_), channel_id=1, source_target_pairs={{0,4},{4,0},{8,12},{12,8},{16,20},{20,16},{24,28},{28,24},{1,5},{5... | collective-permute-start | bytes 786440 | tf_op jit(solution)/shard_map/ppermute | solution.py:63
  90.8 12.7 %copy-start.5 = (bf16[512,256]{1,0:T(8,128)(2,1)}, bf16[512,256]{1,0:T(8,128)(2,1)S(1)}, u32[]{:S(2)}) copy-start(bf16[512,256]{1,0:T(8,128)(2,1)S(1)} %add.79.refs_2_) | copy-start | bytes 786436
  90.8 12.7 %collective-permute-start.5 = (bf16[512,256]{1,0:T(8,128)(2,1)S(1)}, bf16[512,256]{1,0:T(8,128)(2,1)}, u32[]{:S(2)}, u32[]{:S(2)}) collective-permute-start(bf16[512,256]{1,0:T(8,128)(2,1)S(1)} %add.79.refs_2_), channel_id=1, source_target_pairs={{0,4},{4,0},{8,12},{12,8},{16,20},{20,16},{24,28},{28,24},{1,5},{5... | collective-permute-start | bytes 786440 | tf_op jit(solution)/shard_map/ppermute | solution.py:63
  92.4 14.1 %copy-start.6 = (bf16[512,256]{1,0:T(8,128)(2,1)}, bf16[512,256]{1,0:T(8,128)(2,1)S(1)}, u32[]{:S(2)}) copy-start(bf16[512,256]{1,0:T(8,128)(2,1)S(1)} %add.81.refs_6_) | copy-start | bytes 786436
  92.4 14.1 %collective-permute-start.9 = (bf16[512,256]{1,0:T(8,128)(2,1)S(1)}, bf16[512,256]{1,0:T(8,128)(2,1)S(1)}, u32[]{:S(2)}, u32[]{:S(2)}) collective-permute-start(bf16[512,256]{1,0:T(8,128)(2,1)S(1)} %add.81.refs_6_), channel_id=1, source_target_pairs={{0,4},{4,0},{8,12},{12,8},{16,20},{20,16},{24,28},{28,24},{1,5},{5... | collective-permute-start | bytes 786440 | tf_op jit(solution)/shard_map/ppermute | solution.py:63
  93.5 1.3 copy-start.1
  103.6 3.0 %copy-start.13 = (bf16[512,256]{1,0:T(8,128)(2,1)}, bf16[512,256]{1,0:T(8,128)(2,1)S(1)}, u32[]{:S(2)}) copy-start(bf16[512,256]{1,0:T(8,128)(2,1)S(1)} %collective-permute-done.7.refs_5_) | copy-start | bytes 786436
  106.6 0.7 copy-start.14
  125.7 3.0 %copy-start.11 = (f32[128]{0:T(128)S(1)}, f32[128]{0:T(128)}, u32[]{:S(2)}) copy-start(f32[128]{0:T(128)} %param.23) | copy-start | bytes 1540
  125.7 3.7 %copy-start.9 = (f32[128,2]{0,1:T(2,128)S(1)}, f32[128,2]{0,1:T(2,128)}, u32[]{:S(2)}) copy-start(f32[128,2]{0,1:T(2,128)} %param.24) | copy-start | bytes 3076
  125.7 51.7 %all-to-all-start.2 = ((bf16[32,16,2048]{2,1,0:T(8,128)(2,1)}), bf16[32,16,2048]{2,1,0:T(8,128)(2,1)S(1)}, u32[]{:S(2)}, u32[]{:S(2)}) async-start(bf16[32,16,2048]{2,1,0:T(8,128)(2,1)} %bitcast.19), calls=%async_computation.2 | async-start | bytes 4194304 | tf_op jit(solution)/shard_map/all_to_all | solution.py:301
  177.4 1.3 copy-start
